TPU v7x, 512 devices: a whole 4x4x16 slice. The times are simulated.
512 devices in a mesh: kv: 64 (over z, y), tp: 8 (over x, core).
Axes of the slice: x: 4, y: 4, z: 16, core: 2. Of those that a mesh axis runs over, the one named last changes fastest.
Arguments:
- tokens: bfloat16 [64, 4096], P(None, 'kv'), may hold values from -160 to 160
- norm_gain: float32 [4096], P('kv'), may hold values from 0.1 to 1.9
- w_query: bfloat16 [4096, 2048], P('kv', 'tp'), may hold values from -0.09375 to 0.09375
- w_key: bfloat16 [4096, 2048], P('kv', 'tp'), may hold values from -0.5 to 0.5
- w_value: bfloat16 [4096, 2048], P('kv', 'tp'), may hold values from -0.09375 to 0.09375
- w_out: bfloat16 [2048, 4096], P('tp', 'kv'), may hold values from -0.125 to 0.125
- lambdas: float32 [16], P('tp'), may hold values from 0.3 to 0.8
- sub_gain: float32 [128], replicated, may hold values from 0.1 to 1.9
- key_cache: bfloat16 [4, 16, 32768, 128], P(None, 'tp', 'kv'), may hold values from -512 to 512
- value_cache: bfloat16 [4, 16, 32768, 128], P(None, 'tp', 'kv'), may hold values from -6 to 6
- prior: int32 [4], replicated, may hold values from 24576 to 32736
- accepted: int32 [4], replicated, may hold values from 1 to 16
- parent: int32 [4, 16], replicated, may hold values from -1 to 14, as said below
Outputs:
- mixed: bfloat16 [64, 4096], P('tp', 'kv')
- key_out: bfloat16 [4, 16, 32768, 128], P(None, 'tp', 'kv')
- value_out: bfloat16 [4, 16, 32768, 128], P(None, 'tp', 'kv')
Inputs may be any that keep to these rules, and one draw needn't show every extreme that they name: parent[s, 0] is -1, and 0 <= parent[s, j] < j for j >= 1.
All inputs are finite; a program needn't handle non-finite values.
Results may differ from a plain program's by a relative error of at most 0.015.
The roundings to bfloat16 on the way count: a program that leaves them out, or rounds other values in their place, can miss the bound.
Values may be sent and summed in bfloat16 or wider, within the bound.
A program may use at most 64 MiB of HBM per device.

v0:
```python
import math

import jax
import jax.numpy as jnp
from jax import lax
from jax.sharding import Mesh
from jax.sharding import PartitionSpec as P

D = 4096
KV = ("kv_0", "kv_1")


epsilon = 1e-06
masked_score = -1e30
head_scale = 0.8


def in_blocks(array, dim, size):
    shape = array.shape
    pieces = array.reshape(*shape[:dim], size, shape[dim] // size, *shape[dim + 1 :])
    return jnp.moveaxis(pieces, dim, 0)


def sent_and_summed(array, axis, dim):
    size = lax.axis_size(axis)
    pieces = lax.all_to_all(in_blocks(array, dim, size), axis, 0, 0, tiled=True)
    return jnp.sum(pieces, axis=0)


def in_one_piece(arrays, axis, dim, along):
    widths = [math.prod(a.shape[along:]) for a in arrays]
    both = jnp.concatenate(
        [a.reshape(*a.shape[:along], w) for a, w in zip(arrays, widths)], axis=along
    )
    filled = sent_and_summed(both, axis, dim)
    pieces = jnp.split(filled, [sum(widths[:k]) for k in range(1, len(widths))], axis=along)
    return tuple(
        (b.reshape(*filled.shape[:along], *a.shape[along:]) for a, b in zip(arrays, pieces))
    )


def side_by_side(arrays, axis, dim, along):
    ends, at = ([], 0)
    for a in arrays[:-1]:
        at += a.shape[along]
        ends.append(at)
    both = jnp.concatenate(arrays, axis=along)
    return tuple(jnp.split(lax.all_gather(both, axis, axis=dim, tiled=True), ends, axis=along))


def collected_together(array, axis):
    leaves = jax.tree.leaves(array)
    order = sorted(range(len(leaves)), key=lambda k: -leaves[k].size)
    width = (1, *leaves[order[0]].shape)[-1]
    lines = [
        jnp.pad(leaves[k].reshape(-1), (0, -leaves[k].size % width)).reshape(-1, width)
        for k in order
    ]
    both, at, found = (lax.all_gather(jnp.concatenate(lines), axis), 0, {})
    for k, line in zip(order, lines):
        section = both[:, at : at + len(line)].reshape(len(both), -1)
        found[k] = section[:, : leaves[k].size].reshape(-1, *leaves[k].shape)
        at += len(line)
    numbers = iter(range(len(leaves)))
    return jax.tree.map(lambda _: found[next(numbers)], array)


def joined_all(array, axes, combine):
    for axis in axes:
        pieces = collected_together(array, axis)
        array = jax.tree.map(lambda part: part[0], pieces)
        for k in range(1, lax.axis_size(axis)):
            array = combine(array, jax.tree.map(lambda part: part[k], pieces))
    return array


def sum_at_owner(array, axis, dim):
    size = lax.axis_size(axis)
    pieces = lax.all_to_all(in_blocks(array, dim, size), axis, 0, 0, tiled=True)
    return jnp.sum(pieces.astype(jnp.float32), axis=0)


def ancestors(parent):
    prop_count = parent.shape[1]
    identity = jnp.eye(prop_count, dtype=jnp.float32)
    parent_hot = (
        parent[:, :, None] == jnp.arange(prop_count, dtype=jnp.int32)[None, None, :]
    ).astype(jnp.float32)

    def extend(depth_step, ancestry):
        return identity[None] + jnp.einsum("sjm,smi->sji", parent_hot, ancestry)

    return lax.fori_loop(0, prop_count, extend, jnp.broadcast_to(identity, parent_hot.shape))


def combine(earlier, later):
    max_early, totals_early, summed_early = earlier
    max_late, totals_late, summed_late = later
    maximum = jnp.maximum(max_early, max_late)
    factor_early = jnp.exp(max_early - maximum)
    factor_late = jnp.exp(max_late - maximum)
    totals = totals_early * factor_early + totals_late * factor_late
    summed = summed_early * factor_early[..., None] + summed_late * factor_late[..., None]
    return (maximum, totals, summed)


def partial_attend(queries, keys, values, allowed):
    seq_count, head_count, length = (keys.shape[0], keys.shape[1], keys.shape[2])
    head_dim = queries.shape[-1]
    halves = keys.reshape(seq_count, head_count, length, 2, head_dim)
    scores = jnp.einsum(
        "sjhmd,shpmd->mshjp", queries, halves, preferred_element_type=jnp.float32
    ) * head_dim ** (-0.5)
    visible = allowed[None, :, None, :, :]
    maximum = jnp.max(jnp.where(visible, scores, masked_score), axis=-1)
    weight = jnp.where(visible, jnp.exp(scores - maximum[..., None]), 0.0)
    totals = jnp.sum(weight, axis=-1)
    summed = jnp.einsum(
        "mshjp,shpc->mshjc", weight.astype(jnp.bfloat16), values, preferred_element_type=jnp.float32
    )
    return (maximum, totals, summed)


def body(
    tokens,
    norm_gain,
    w_query,
    w_key,
    w_value,
    w_out,
    lambdas,
    sub_gain,
    key_cache,
    value_cache,
    prior,
    accepted,
    parent,
):
    seq_count, prop_count = parent.shape
    head_count = lambdas.shape[0]
    head_dim = w_query.shape[1] // (2 * head_count)
    value_dim = sub_gain.shape[0]
    length = key_cache.shape[2]
    as_float = tokens.astype(jnp.float32)
    row_squares = jnp.sum(as_float * as_float, axis=1)
    normed = (as_float * norm_gain[None, :]).astype(jnp.bfloat16)
    part_query = jnp.dot(normed, w_query, preferred_element_type=jnp.float32)
    part_key = jnp.dot(normed, w_key, preferred_element_type=jnp.float32)
    part_value = jnp.dot(normed, w_value, preferred_element_type=jnp.float32)
    sum_query, sum_key, sum_value, sum_squares = in_one_piece(
        (part_query, part_key, part_value, row_squares), KV, 0, 1
    )
    row_scale = lax.rsqrt(sum_squares / D + epsilon)[:, None]
    own_query = (row_scale * sum_query).astype(jnp.bfloat16)
    own_key = (row_scale * sum_key).astype(jnp.bfloat16)
    own_value = (row_scale * sum_value).astype(jnp.bfloat16)
    queries, new_key, new_value = side_by_side((own_query, own_key, own_value), KV, 0, 1)
    queries = queries.reshape(seq_count, prop_count, head_count, 2, head_dim)
    new_key = new_key.reshape(seq_count, prop_count, head_count, 2 * head_dim).transpose(0, 2, 1, 3)
    new_value = new_value.reshape(seq_count, prop_count, head_count, value_dim).transpose(
        0, 2, 1, 3
    )
    valid_end = prior + accepted
    positions = lax.axis_index(KV) * length + jnp.arange(length, dtype=jnp.int32)
    offset_in = positions[None, :] - valid_end[:, None]
    one_hot = offset_in[:, :, None] == jnp.arange(prop_count, dtype=jnp.int32)[None, None, :]
    inside = (offset_in >= 0) & (offset_in < prop_count)
    hot_rows = one_hot.astype(jnp.bfloat16)
    placed_key = jnp.einsum(
        "spj,shjc->shpc", hot_rows, new_key, preferred_element_type=jnp.float32
    ).astype(jnp.bfloat16)
    placed_value = jnp.einsum(
        "spj,shjc->shpc", hot_rows, new_value, preferred_element_type=jnp.float32
    ).astype(jnp.bfloat16)
    key_out = jnp.where(inside[:, None, :, None], placed_key, key_cache)
    value_out = jnp.where(inside[:, None, :, None], placed_value, value_cache)
    ancestry = ancestors(parent)
    settled = offset_in < 0
    in_tree = jnp.einsum("sjm,spm->sjp", ancestry, one_hot.astype(jnp.float32)) > 0.5
    allowed = settled[:, None, :] | in_tree
    shard_keys, shard_values = (key_out, value_out)
    local_terms = partial_attend(queries, shard_keys, shard_values, allowed)
    merged = joined_all(local_terms, KV, combine)
    maximum, totals, summed = merged
    head_out = (
        summed[0] / totals[0][..., None]
        - lambdas[None, :, None, None] * summed[1] / totals[1][..., None]
    )
    mean_square = jnp.mean(head_out * head_out, axis=-1, keepdims=True)
    attended = (head_out * lax.rsqrt(mean_square + epsilon) * sub_gain * head_scale).astype(
        jnp.bfloat16
    )
    attended = attended.transpose(0, 2, 1, 3).reshape(
        seq_count * prop_count, head_count * value_dim
    )
    partial_value = jnp.dot(attended, w_out, preferred_element_type=jnp.float32).astype(
        jnp.bfloat16
    )
    mixed = sum_at_owner(partial_value.astype(jnp.float32).astype(jnp.bfloat16), "tp", 0).astype(
        jnp.bfloat16
    )
    return (mixed, key_out, value_out)


def solution(mesh):
    finer = Mesh(mesh.devices.reshape(16, 4, mesh.shape["tp"]), ("kv_0", "kv_1", "tp"))
    in_specs = (
        P(None, KV),
        P(KV),
        P(KV, "tp"),
        P(KV, "tp"),
        P(KV, "tp"),
        P("tp", KV),
        P("tp"),
        P(),
        P(None, "tp", KV, None),
        P(None, "tp", KV, None),
        P(),
        P(),
        P(),
    )
    out_specs = (P("tp", KV), P(None, "tp", KV, None), P(None, "tp", KV, None))
    return jax.shard_map(body, mesh=finer, in_specs=in_specs, out_specs=out_specs, check_vma=False)
```

profile of v0, /device:TPU:1, one launch (start us, length us, event | category | flops | bytes accessed | tf_op | source)
XLA Modules:
  0.0 243.6 jit_solution(17906228244786038245)
XLA Ops:
  7.2 0.9 fusion.75
  8.1 0.8 fusion.83
  9.0 0.9 fusion.85
  9.9 0.9 fusion.87
  10.8 0.1 copy.73
  10.9 0.9 copy.74
  11.9 19.3 %all-to-all-start = ((f32[64,1,769]{2,1,0:T(1,128)}), f32[64,1,769]{2,1,0:T(1,128)S(1)}, u32[]{:S(2)}, u32[]{:S(2)}) async-start(f32[64,1,769]{2,1,0:T(1,128)} %copy.74), calls=%async_computation | async-start | bytes 458752 | tf_op jit(solution)/shard_map/all_to_all | solution.py:26
  31.2 0.5 copy.78
  31.8 3.4 %while.11 = (s32[]{:T(128)}, bf16[4,16,16]{2,1,0:T(8,128)(2,1)S(1)}, s32[4,16]{1,0:T(4,128)S(1)}, s32[]{:T(128)}) while((s32[]{:T(128)}, bf16[4,16,16]{2,1,0:T(8,128)(2,1)S(1)}, s32[4,16]{1,0:T(4,128)S(1)}, s32[]{:T(128)}) %tuple.96), condition=%wide.region_3.4_spmd.clone, body=%wide.region_2.3_spmd.clone.sunk | while | flops 37378 | bytes 10549 | solution.py:93
  31.8 0.2 convolution_add_fusion.2
  32.0 0.2 convolution_add_fusion.2
  32.3 0.2 convolution_add_fusion.2
  32.5 0.2 convolution_add_fusion.2
  32.7 0.2 convolution_add_fusion.2
  32.9 0.2 convolution_add_fusion.2
  33.1 0.2 convolution_add_fusion.2
  33.3 0.2 convolution_add_fusion.2
  33.5 0.2 convolution_add_fusion.2
  33.7 0.2 convolution_add_fusion.2
  33.9 0.2 convolution_add_fusion.2
  34.1 0.2 convolution_add_fusion.2
  34.4 0.2 convolution_add_fusion.2
  34.6 0.2 convolution_add_fusion.2
  34.8 0.2 convolution_add_fusion.2
  35.0 0.2 convolution_add_fusion.2
  35.2 1.5 copy.76
  36.9 0.2 fusion.11
  37.0 12.5 %all-to-all-done = f32[64,1,769]{2,1,0:T(1,128)S(1)} async-done(((f32[64,1,769]{2,1,0:T(1,128)}), f32[64,1,769]{2,1,0:T(1,128)S(1)}, u32[]{:S(2)}, u32[]{:S(2)}) %all-to-all-start) | async-done | bytes 196896 | tf_op jit(solution)/shard_map/all_to_all | solution.py:26
  49.6 0.2 reduce_sum.51
  49.7 0.5 split.28
  51.0 62.2 %all-gather.2 = bf16[64,1,768]{2,1,0:T(2,128)(2,1)S(1)} all-gather(bf16[1,1,768]{2,1,0:T(2,128)(2,1)S(1)} %maximum_bitcast_fusion.3), channel_id=1, replica_groups=mesh['kv_0'=16,'kv_1'=4,'tp'=8] {'kv_0','kv_1'}, dimensions={0}, use_global_device_ids=true | all-gather | bytes 99840 | tf_op jit(solution)/shard_map/all_gather | solution.py:48
  113.2 0.1 reshape.1444
  113.3 0.5 fusion.10
  113.8 0.3 select_reduce_fusion
  114.1 0.1 reshape.1448
  114.2 0.3 fusion.16
  114.5 0.5 fusion.8
  115.0 0.4 convolution_bitcast_fusion
  115.5 0.1 reshape.1449
  115.6 0.7 maximum_bitcast_fusion.1
  116.3 76.6 %all-gather.7.cloned.1.call-done = f32[16,260,128]{2,1,0:T(8,128)} async-done(((f32[1,260,128]{2,1,0:T(8,128)}), f32[16,260,128]{2,1,0:T(8,128)}) %all-gather.7.cloned.1.call-update) | async-done | bytes 2129936 | tf_op jit(solution)/shard_map/all_gather | solution.py:59
  192.9 0.7 fusion.173
  193.5 0.9 fusion.96
  194.5 0.7 fusion.172
  195.2 0.7 fusion.170
  195.9 0.7 fusion.168
  196.6 0.7 fusion.166
  197.3 0.7 fusion.164
  198.0 0.7 fusion.162
  198.7 0.7 fusion.160
  199.4 2.6 %fusion.19 = f32[256,128]{1,0:T(8,128)S(1)} fusion(f32[16,260,128]{2,1,0:T(8,128)} %all-gather.7.cloned.1.call-done, f32[256]{0:T(256)S(1)} %get-tuple-element.113, f32[256]{0:T(256)S(1)} %get-tuple-element.110, f32[256]{0:T(256)S(1)} %get-tuple-element.112, f32[256]{0:T(256)S(1)} %get-tuple-element.111, f32[256]{0:T(256)S(1)} %get-tuple-element.109, ...), kind=kLoop, calls=%fused_computation.32 | loop fusion | flops 1474560 | bytes 2258944 | tf_op jit(solution)/shard_map/add | solution.py:103
  202.1 10.2 %all-gather.4 = f32[4,260,128]{2,1,0:T(8,128)S(1)} all-gather(f32[1,260,128]{2,1,0:T(8,128)S(1)} %maximum_bitcast_fusion.2), channel_id=3, replica_groups=mesh['kv_0'=16,'kv_1'=4,'tp'=8] {'kv_1'}, dimensions={0}, use_global_device_ids=true | all-gather | bytes 665600 | tf_op jit(solution)/shard_map/all_gather | solution.py:59
  212.3 0.1 squeeze.294
  213.1 0.3 multiply_add_fusion
  213.4 0.2 multiply_reduce_fusion
  213.6 0.1 fusion.76
  213.8 0.1 fusion.12
  213.9 0.7 reshape.1464
  214.6 16.9 %all-to-all-start.1 = ((bf16[8,2,256]{2,1,0:T(2,128)(2,1)}), bf16[8,2,256]{2,1,0:T(2,128)(2,1)S(1)}, u32[]{:S(2)}, u32[]{:S(2)}) async-start(bf16[8,2,256]{2,1,0:T(2,128)(2,1)} %reshape.1464), calls=%async_computation.1 | async-start | bytes 16384 | tf_op jit(solution)/shard_map/all_to_all | solution.py:79
  231.5 1.3 copy.86
  232.8 1.3 copy.85
  234.1 2.0 all-to-all-done.1
  236.1 0.1 reshape.1465
  236.2 0.6 reduce_sum.55
  (79 shorter events, 1.3 us)
Async XLA Ops:
  7.2 1.0 copy-start
  7.2 24.0 %copy-start.1 = (bf16[4,2,512,128]{3,2,1,0:T(8,128)(2,1)S(1)}, bf16[4,2,512,128]{3,2,1,0:T(8,128)(2,1)}, u32[]{:S(2)}) copy-start(bf16[4,2,512,128]{3,2,1,0:T(8,128)(2,1)} %param.23) | copy-start | bytes 3145732
  7.2 24.6 %copy-start.5 = (s32[4,16]{1,0:T(4,128)S(1)}, s32[4,16]{1,0:T(4,128)}, u32[]{:S(2)}) copy-start(s32[4,16]{1,0:T(4,128)} %param.27) | copy-start | bytes 772
  11.9 37.7 %all-to-all-start = ((f32[64,1,769]{2,1,0:T(1,128)}), f32[64,1,769]{2,1,0:T(1,128)S(1)}, u32[]{:S(2)}, u32[]{:S(2)}) async-start(f32[64,1,769]{2,1,0:T(1,128)} %copy.74), calls=%async_computation | async-start | bytes 458752 | tf_op jit(solution)/shard_map/all_to_all | solution.py:26
  31.1 161.7 %all-gather.7.cloned.1.call-start = ((), (), s32[]{:S(2)}) async-start(), calls=%async_computation.2 | async-start | bytes 2297856 | tf_op jit(solution)/shard_map/all_gather | solution.py:59
  31.2 5.5 %copy-start.6 = (s32[4]{0:T(128)S(1)}, s32[4]{0:T(128)}, u32[]{:S(2)}) copy-start(s32[4]{0:T(128)} %param.25) | copy-start | bytes 52
  31.2 5.5 %copy-start.7 = (s32[4]{0:T(128)S(1)}, s32[4]{0:T(128)}, u32[]{:S(2)}) copy-start(s32[4]{0:T(128)} %param.26) | copy-start | bytes 52
  199.4 14.0 %copy-start.3 = (f32[2]{0:T(128)S(1)}, f32[2]{0:T(128)}, u32[]{:S(2)}) copy-start(f32[2]{0:T(128)} %param.21) | copy-start | bytes 28
  202.0 11.6 %copy-start.4 = (f32[128]{0:T(128)S(1)}, f32[128]{0:T(128)}, u32[]{:S(2)}) copy-start(f32[128]{0:T(128)} %param.22) | copy-start | bytes 1540
  202.0 11.7 %copy-start.2 = (bf16[256,64]{0,1:T(8,128)(2,1)S(1)}, bf16[256,64]{0,1:T(8,128)(2,1)}, u32[]{:S(2)}) copy-start(bf16[256,64]{0,1:T(8,128)(2,1)} %param.20) | copy-start | bytes 98308
  214.6 21.5 %all-to-all-start.1 = ((bf16[8,2,256]{2,1,0:T(2,128)(2,1)}), bf16[8,2,256]{2,1,0:T(2,128)(2,1)S(1)}, u32[]{:S(2)}, u32[]{:S(2)}) async-start(bf16[8,2,256]{2,1,0:T(2,128)(2,1)} %reshape.1464), calls=%async_computation.1 | async-start | bytes 16384 | tf_op jit(solution)/shard_map/all_to_all | solution.py:79
Sparse Core Ops, SparseCore 0:
  116.4 76.4 all-gather.6
where the time goes:
time: 245 us; the launch traced here: 244 us
  waiting for transfers between devices  91.1 us (37%)
  blocking collectives  72.4 us (30%)
  starting transfers between devices  36.2 us (15%)
  between operations  15.1 us (6%)
  other arithmetic  12.6 us (5%)
  local copies, waits for them, and re-layouts  8.21 us (3%)
  matrix products  7.78 us (3%)
    all_gather x1, waiting for transfers between devices, collected_together(): both, at, found = (lax.all_gather(jnp.concatenate(lines), axis), 0, {})  76.6 us
    all_gather x1, blocking collectives, side_by_side(): lax.all_gather(both, axis, axis=dim, tiled=True)  62.2 us
    all_to_all x1, starting transfers between devices, sent_and_summed(): pieces = lax.all_to_all(in_blocks(array, dim, size), axis, 0, 0, tiled=True)  19.3 us
    all_to_all x1, starting transfers between devices, sum_at_owner(): pieces = lax.all_to_all(in_blocks(array, dim, size), axis, 0, 0, tiled=True)  16.9 us
    all_to_all x1, waiting for transfers between devices, sent_and_summed(): pieces = lax.all_to_all(in_blocks(array, dim, size), axis, 0, 0, tiled=True)  12.5 us
    all_gather x1, blocking collectives, collected_together(): both, at, found = (lax.all_gather(jnp.concatenate(lines), axis), 0, {})  10.2 us
    unnamed x23, local copies, waits for them, and re-layouts  5.48 us
    exp x7, other arithmetic, combine(): factor_late = jnp.exp(max_late - maximum)  4.92 us
  transfers between devices with their start and end apart: 3, of which 3 were waited for; matrix products, arithmetic and copies ran while one was open for 3% of the time, Pallas kernels for 0%

commit v1 on v0

v1 whole, which is shorter than its diff:
```python
import functools

import jax
import jax.numpy as jnp
from jax import lax
from jax.experimental import pallas as pl
from jax.experimental.pallas import tpu as pltpu
from jax.sharding import PartitionSpec as P

MESH = pl.DeviceIdType.MESH
VMEM = pl.BlockSpec(memory_space=pltpu.VMEM)
SMEM = pl.BlockSpec(memory_space=pltpu.SMEM)
HBM = pl.BlockSpec(memory_space=pl.ANY)

D = 4096
NZ, NY, NT = 16, 4, 8
SEQS, PROPS, TOKENS = 4, 16, 64
EPS = 1e-06
MASKED = -1e30
HEAD_SCALE = 0.8
F32, BF16 = jnp.float32, jnp.bfloat16


def z_step(k):
    odd = lax.rem(k, 2)
    return 8 + odd * lax.div(k + 1, 2) - (1 - odd) * lax.div(k, 2)


def to_plane(z, y, tp, send):
    def far(i, carry):
        tz = lax.rem(z + z_step(lax.div(i, NY)), NZ)
        ty = lax.rem(y + lax.rem(i, NY), NY)
        send(tz, ty)
        return carry

    lax.fori_loop(0, (NZ - 1) * NY, far, 0)

    def near(i, carry):
        send(z, lax.rem(y + i, NY))
        return carry

    lax.fori_loop(1, NY, near, 0)


def wait_bytes(ref, count, sem):
    piece = ref.at[pl.ds(0, count)]
    pltpu.make_async_copy(piece, piece, sem).wait()


def split3(x):
    high = x.astype(BF16).astype(F32)
    rest = x - high
    mid = rest.astype(BF16).astype(F32)
    return high, mid, (rest - mid).astype(BF16).astype(F32)


def fused(
    tok_ref, gain_ref, wq_ref, wk_ref, wv_ref, wo_ref, lam_ref, sub_ref, prior_ref, acc_ref, par_ref, kc_ref, vc_ref,
    mixed_ref, nk_ref, nv_ref,
    kbuf, vbuf, part, yb, zsrc, zb, ag, rows, terms, csrc, cb, cterms, att, attf, psrc, pb,
    load_sem, y_send, y_recv, z_send, z_recv, a_send, a_recv, c_send, c_recv, t_send, t_recv, p_send, p_recv,
):
    kv, tp = lax.axis_index("kv"), lax.axis_index("tp")
    z, y = lax.div(kv, NY), lax.rem(kv, NY)
    mine = y * NZ + z
    length = kbuf.shape[2]

    load_k = pltpu.make_async_copy(kc_ref, kbuf, load_sem.at[0])
    load_v = pltpu.make_async_copy(vc_ref, vbuf, load_sem.at[1])

    barrier = pltpu.get_barrier_semaphore()

    def greet(tz, ty):
        pl.semaphore_signal(barrier, inc=1, device_id=(tz * NY + ty, tp), device_id_type=MESH)

    to_plane(z, y, tp, greet)

    def greet_tp(i, carry):
        pl.semaphore_signal(barrier, inc=1, device_id=(kv, lax.rem(tp + i, NT)), device_id_type=MESH)
        return carry

    lax.fori_loop(1, NT, greet_tp, 0)
    load_k.start()
    load_v.start()

    x = tok_ref[...].astype(F32)
    normed = (x * gain_ref[...]).astype(BF16)
    squares = jnp.sum(x * x, axis=1, keepdims=True)
    for c, w in enumerate((wq_ref, wk_ref, wv_ref)):
        product = jnp.dot(normed, w[...], preferred_element_type=F32)
        part[:, 2 * c, :] = product[:, :128]
        part[:, 2 * c + 1, :] = product[:, 128:]
    part[:, 6, :] = jnp.broadcast_to(squares, (TOKENS, 128))

    at_i = lax.broadcasted_iota(jnp.int32, (PROPS, PROPS), 0)
    at_j = lax.broadcasted_iota(jnp.int32, (PROPS, PROPS), 1)
    twice_j = lax.rem(lax.broadcasted_iota(jnp.int32, (2 * PROPS, PROPS), 0), PROPS)
    twice_i = lax.broadcasted_iota(jnp.int32, (2 * PROPS, PROPS), 1)
    twice = jnp.where(twice_j == twice_i, 1.0, 0.0).astype(BF16)
    ancestry = []
    for s in range(SEQS):
        parents = par_ref[s : s + 1, :]
        reach = jnp.where((at_i == parents) | (at_i == at_j), 1.0, 0.0)
        for _ in range(4):
            step = reach.astype(BF16)
            reach = jnp.where(jnp.dot(step, step, preferred_element_type=F32) > 0.5, 1.0, 0.0)
        ancestry.append(
            lax.dot_general(twice, reach.astype(BF16), (((1,), (1,)), ((), ())), preferred_element_type=F32)
        )

    pl.semaphore_wait(barrier, NZ * NY - 1 + NT - 1)

    for step in (2, 1, 3):
        ty = lax.rem(y + step, NY)
        pltpu.make_async_remote_copy(
            part.at[pl.ds(ty * NZ, NZ)], yb.at[y], y_send, y_recv, device_id=(z * NY + ty, tp), device_id_type=MESH
        ).start()
    yb[y] = part[pl.ds(y * NZ, NZ)]
    wait_bytes(yb, NY - 1, y_recv)
    zsrc[...] = (yb[0] + yb[1]) + (yb[2] + yb[3])

    def send_z(k, carry):
        tz = lax.rem(z + z_step(k), NZ)
        pltpu.make_async_remote_copy(
            zsrc.at[tz], zb.at[z], z_send, z_recv, device_id=(tz * NY + y, tp), device_id_type=MESH
        ).start()
        return carry

    lax.fori_loop(0, NZ - 1, send_z, 0)
    zb[z] = zsrc[z]
    wait_bytes(zb, NZ - 1, z_recv)
    total = jnp.sum(zb[...], axis=0)
    scale = lax.rsqrt(total[6:7, :] / D + EPS)
    ag[mine] = (total[:6, :] * scale).astype(BF16)

    def send_a(tz, ty):
        pltpu.make_async_remote_copy(
            ag.at[mine], ag.at[mine], a_send, a_recv, device_id=(tz * NY + ty, tp), device_id_type=MESH
        ).start()

    to_plane(z, y, tp, send_a)
    load_k.wait()
    load_v.wait()
    wait_bytes(ag, NZ * NY - 1, a_recv)
    rows[...] = ag[...].astype(F32)

    base = kv * length
    lane = lax.broadcasted_iota(jnp.int32, (PROPS, 128), 1)
    position = lax.broadcasted_iota(jnp.int32, (2 * PROPS, length), 1) + base
    tree_at = lax.broadcasted_iota(jnp.int32, (2 * PROPS, PROPS), 1) - base
    contract_last = (((1,), (1,)), ((), ()))
    for s in range(SEQS):
        end = prior_ref[s] + acc_ref[s]
        settled = position < end
        placed = tree_at + end
        in_tree = (ancestry[s] > 0.5) & (placed >= 0) & (placed < length)
        tokens = slice(s * PROPS, (s + 1) * PROPS)
        stats = jnp.zeros((PROPS, 128), F32)
        for h in range(2):
            q = rows[tokens, h, :]
            both = jnp.concatenate([jnp.where(lane < 64, q, 0.0), jnp.where(lane < 64, 0.0, q)], axis=0).astype(BF16)
            new_k = rows[tokens, 2 + h, :].astype(BF16)
            new_v = rows[tokens, 4 + h, :].astype(BF16)
            nk_ref[s, h] = new_k
            nv_ref[s, h] = new_v
            scores = lax.dot_general(both, kbuf[s, h], contract_last, preferred_element_type=F32) * 0.125
            tree = lax.dot_general(both, new_k, contract_last, preferred_element_type=F32) * 0.125
            maximum = jnp.maximum(
                jnp.max(jnp.where(settled, scores, MASKED), axis=1, keepdims=True),
                jnp.max(jnp.where(in_tree, tree, MASKED), axis=1, keepdims=True),
            )
            weight = jnp.where(settled, jnp.exp(scores - maximum), 0.0)
            tree_weight = jnp.where(in_tree, jnp.exp(tree - maximum), 0.0)
            totals = jnp.sum(weight, axis=1, keepdims=True) + jnp.sum(tree_weight, axis=1, keepdims=True)
            summed = jnp.dot(weight.astype(BF16), vbuf[s, h], preferred_element_type=F32) + jnp.dot(
                tree_weight.astype(BF16), new_v, preferred_element_type=F32
            )
            for m in range(2):
                c = 2 * m + h
                half = slice(m * PROPS, (m + 1) * PROPS)
                terms[tokens, c, :] = summed[half]
                for n, column in ((c, maximum[half]), (4 + c, totals[half])):
                    for k, piece in enumerate(split3(column)):
                        stats = jnp.where(lane == 8 * k + n, piece, stats)
        terms[tokens, 4, :] = stats
        terms[tokens, 5, :] = jnp.zeros((PROPS, 128), F32)
    csrc[...] = terms[...].astype(BF16)

    def send_c(tz, ty):
        pltpu.make_async_remote_copy(
            csrc.at[ty * NZ + tz], cb.at[mine], c_send, c_recv, device_id=(tz * NY + ty, tp), device_id_type=MESH
        ).start()

    to_plane(z, y, tp, send_c)
    cb[mine] = csrc[mine]
    wait_bytes(cb, NZ * NY - 1, c_recv)
    cterms[...] = cb[...].astype(F32)

    st = cterms[:, 4, :]
    heads = []
    for c in range(4):
        maxima = (st[:, c : c + 1] + st[:, 8 + c : 9 + c]) + st[:, 16 + c : 17 + c]
        shares = (st[:, 4 + c : 5 + c] + st[:, 12 + c : 13 + c]) + st[:, 20 + c : 21 + c]
        factor = jnp.exp(maxima - jnp.max(maxima, axis=0, keepdims=True))
        whole = jnp.sum(factor * shares, axis=0, keepdims=True)
        heads.append(jnp.sum(factor * cterms[:, c, :], axis=0, keepdims=True) / whole)
    attended = []
    for h in range(2):
        head_out = heads[h] - lam_ref[h] * heads[2 + h]
        square = jnp.mean(head_out * head_out, axis=1, keepdims=True)
        attended.append(head_out * lax.rsqrt(square + EPS) * sub_ref[...] * HEAD_SCALE)
    att[mine] = jnp.concatenate(attended, axis=0).astype(BF16)

    def send_t(tz, ty):
        pltpu.make_async_remote_copy(
            att.at[mine], att.at[mine], t_send, t_recv, device_id=(tz * NY + ty, tp), device_id_type=MESH
        ).start()

    to_plane(z, y, tp, send_t)
    psrc[...] = jnp.zeros(psrc.shape, F32)
    wait_bytes(att, NZ * NY - 1, t_recv)
    attf[...] = att[...].astype(F32)

    out = jnp.dot(attf[:, 0, :].astype(BF16), wo_ref[:128, :], preferred_element_type=F32) + jnp.dot(
        attf[:, 1, :].astype(BF16), wo_ref[128:, :], preferred_element_type=F32
    )
    psrc[:, :, :64] = out.astype(BF16).astype(F32).reshape(NT, TOKENS // NT, 64)

    def send_p(i, carry):
        other = lax.rem(tp + i, NT)
        pltpu.make_async_remote_copy(
            psrc.at[other], pb.at[tp], p_send, p_recv, device_id=(kv, other), device_id_type=MESH
        ).start()
        return carry

    lax.fori_loop(1, NT, send_p, 0)
    pb[tp] = psrc[tp]
    wait_bytes(yb, NY - 1, y_send)
    wait_bytes(zb, NZ - 1, z_send)
    wait_bytes(ag, NZ * NY - 1, a_send)
    wait_bytes(cb, NZ * NY - 1, c_send)
    wait_bytes(att, NZ * NY - 1, t_send)
    wait_bytes(pb, NT - 1, p_recv)
    wait_bytes(pb, NT - 1, p_send)
    mixed_ref[...] = jnp.sum(pb[...], axis=0)[:, :64].astype(BF16)


def insert(prior_ref, acc_ref, nk_ref, nv_ref, k_ref, v_ref, ko_ref, vo_ref):
    s = pl.program_id(0)
    length = k_ref.shape[2]
    end = prior_ref[s] + acc_ref[s] - lax.axis_index("kv") * length
    offset = lax.broadcasted_iota(jnp.int32, (length, PROPS), 0) - end
    hot = jnp.where(offset == lax.broadcasted_iota(jnp.int32, (length, PROPS), 1), 1.0, 0.0).astype(BF16)
    across = lax.broadcasted_iota(jnp.int32, (length, 128), 0) - end
    inside = (across >= 0) & (across < PROPS)
    for new, old, out in ((nk_ref, k_ref, ko_ref), (nv_ref, v_ref, vo_ref)):
        for h in range(2):
            placed = jnp.dot(hot, new[0, h], preferred_element_type=F32)
            out[0, h] = jnp.where(inside, placed, old[0, h].astype(F32)).astype(BF16)


def body(
    tokens, norm_gain, w_query, w_key, w_value, w_out, lambdas, sub_gain, key_cache, value_cache, prior, accepted, parent
):
    length = key_cache.shape[2]
    new_rows = jax.ShapeDtypeStruct((SEQS, 2, PROPS, 128), BF16)
    mixed, new_key, new_value = pl.pallas_call(
        fused,
        name="fused",
        out_shape=(jax.ShapeDtypeStruct((TOKENS // NT, 64), BF16), new_rows, new_rows),
        in_specs=[VMEM] * 6 + [SMEM, VMEM, SMEM, SMEM, VMEM, HBM, HBM],
        out_specs=(VMEM,) * 3,
        scratch_shapes=[
            pltpu.VMEM((SEQS, 2, length, 128), BF16),
            pltpu.VMEM((SEQS, 2, length, 128), BF16),
            pltpu.VMEM((TOKENS, 7, 128), F32),
            pltpu.VMEM((NY, NZ, 7, 128), F32),
            pltpu.VMEM((NZ, 7, 128), F32),
            pltpu.VMEM((NZ, 7, 128), F32),
            pltpu.VMEM((TOKENS, 6, 128), BF16),
            pltpu.VMEM((TOKENS, 6, 128), F32),
            pltpu.VMEM((TOKENS, 6, 128), F32),
            pltpu.VMEM((TOKENS, 6, 128), BF16),
            pltpu.VMEM((TOKENS, 6, 128), BF16),
            pltpu.VMEM((TOKENS, 6, 128), F32),
            pltpu.VMEM((TOKENS, 2, 128), BF16),
            pltpu.VMEM((TOKENS, 2, 128), F32),
            pltpu.VMEM((NT, TOKENS // NT, 128), F32),
            pltpu.VMEM((NT, TOKENS // NT, 128), F32),
            pltpu.SemaphoreType.DMA((2,)),
        ]
        + [pltpu.SemaphoreType.DMA] * 12,
        compiler_params=pltpu.CompilerParams(collective_id=0, has_side_effects=True),
    )(
        tokens, norm_gain.reshape(1, -1), w_query, w_key, w_value, w_out, lambdas, sub_gain.reshape(1, -1),
        prior, accepted, parent, key_cache, value_cache,
    )
    rows = pl.BlockSpec((1, 2, PROPS, 128), lambda s: (s, 0, 0, 0))
    shard = pl.BlockSpec((1, 2, length, 128), lambda s: (s, 0, 0, 0))
    cache = jax.ShapeDtypeStruct(key_cache.shape, BF16)
    key_out, value_out = pl.pallas_call(
        insert,
        name="insert",
        grid=(SEQS,),
        out_shape=(cache, cache),
        in_specs=[SMEM, SMEM, rows, rows, shard, shard],
        out_specs=(shard, shard),
    )(prior, accepted, new_key, new_value, key_cache, value_cache)
    return mixed, key_out, value_out


def solution(mesh):
    in_specs = (
        P(None, "kv"),
        P("kv"),
        P("kv", "tp"),
        P("kv", "tp"),
        P("kv", "tp"),
        P("tp", "kv"),
        P("tp"),
        P(),
        P(None, "tp", "kv", None),
        P(None, "tp", "kv", None),
        P(),
        P(),
        P(),
    )
    out_specs = (P("tp", "kv"), P(None, "tp", "kv", None), P(None, "tp", "kv", None))
    return jax.shard_map(body, mesh=mesh, in_specs=in_specs, out_specs=out_specs, check_vma=False)
```

time: 245 us -> 71.8 us (0.29)
  waiting for transfers between devices: 91.1 us -> 0 us
  blocking collectives: 72.4 us -> 0 us
  Pallas kernels: 0 us -> 68 us
  starting transfers between devices: 36.2 us -> 0 us
  between operations: 15.1 us -> 0.64 us
  other arithmetic: 12.6 us -> 0 us
  matrix products: 7.78 us -> 0 us
  local copies, waits for them, and re-layouts: 8.21 us -> 2.75 us
    all_gather x1 -> x0, waiting for transfers between devices: 76.6 us -> none  [collected_together(): both, at, found = (lax.all_gather(jnp.concatenate(lines), axis), 0, {})]
    all_gather x2 -> x0, blocking collectives: 72.4 us -> none  [the longest x1 62.2 us: side_by_side(): lax.all_gather(both, axis, axis=dim, tiled=True)]
    pallas_call x0 -> x2, Pallas kernels: none -> 68 us  [the longest x1 63.8 us: body(): pl.pallas_call(fused, name='fused', out_shape=(jax.ShapeDtypeStruct((TOKE...]
    all_to_all x2 -> x0, starting transfers between devices: 36.1 us -> none  [the longest x1 19.3 us: sent_and_summed(): pieces = lax.all_to_all(in_blocks(array, dim, size), axis, 0, 0, tiled=True)]
    all_to_all x2 -> x0, waiting for transfers between devices: 14.5 us -> none  [the longest x1 12.5 us: sent_and_summed(): pieces = lax.all_to_all(in_blocks(array, dim, size), axis, 0, 0, tiled=True)]
    dot_general x25 -> x0, matrix products: 7.78 us -> none  [the longest x16 3.07 us: extend(): return identity[None] + jnp.einsum('sjm,smi->sji', parent_hot, ancestry)]
    exp x8 -> x0, other arithmetic: 5.61 us -> none  [the longest x7 4.92 us: combine(): factor_late = jnp.exp(max_late - maximum)]
    add x6 -> x0, other arithmetic: 3.83 us -> none  [the longest x2 2.86 us: combine(): summed_early * factor_early[..., None]]
  transfers between devices with their start and end apart: 3 -> 0, of which waited for: 3 -> 0; matrix products, arithmetic and copies ran while one was open for 3% -> 0% of each run, Pallas kernels for 0% -> 0%
where the time goes in v1:
time: 71.8 us; the launch traced here: 71.4 us
  Pallas kernels  68 us (95%)
  local copies, waits for them, and re-layouts  2.75 us (4%)
    pallas_call x1, Pallas kernels, body(): pl.pallas_call(fused, name='fused', out_shape=(jax.ShapeDtypeStruct((TOKE...  63.8 us
    pallas_call x1, Pallas kernels, body(): pl.pallas_call(insert, name='insert', grid=(SEQS,), out_shape=(cache, cac...  4.22 us
    unnamed x4, local copies, waits for them, and re-layouts  2.75 us

profile of v1, /device:TPU:1, one launch (start us, length us, event | category | flops | bytes accessed | tf_op | source)
XLA Modules:
  0.0 71.4 jit_solution(1970095777913826697)
XLA Ops:
  0.6 1.5 %copy.16.wo_ref = bf16[256,64]{1,0:T(8,128)(2,1)} copy(bf16[256,64]{0,1:T(8,128)(2,1)} %param.18) | data formatting | bytes 65536 | tf_op args[5]
  2.1 63.8 %fused.1 = (bf16[8,64]{1,0:T(8,128)(2,1)}, bf16[4,2,16,128]{3,2,1,0:T(8,128)(2,1)}, bf16[4,2,16,128]{3,2,1,0:T(8,128)(2,1)}) custom-call(bf16[64,64]{1,0:T(8,128)(2,1)} %tok_ref.1, f32[1,64]{1,0:T(1,128)} %bitcast.2, bf16[64,256]{1,0:T(8,128)(2,1)} %wq_ref.1, bf16[64,256]{1,0:T(8,128)(2,1)} %wk_ref.1, bf16[64,256]{1,0:T(8,128)(2,1)} %wv_ref.1, ...), custom_call_target="tpu_custom_call" | custom-call | tf_op jit(solution)/shard_map/fused/pallas_call | solution.py:267
  66.0 4.2 %insert.1 = (bf16[4,2,512,128]{3,2,1,0:T(8,128)(2,1)}, bf16[4,2,512,128]{3,2,1,0:T(8,128)(2,1)}) custom-call(s32[4]{0:T(128)} %prior_ref.3, s32[4]{0:T(128)} %acc_ref.3, bf16[4,2,16,128]{3,2,1,0:T(8,128)(2,1)} %get-tuple-element.9.nk_ref, bf16[4,2,16,128]{3,2,1,0:T(8,128)(2,1)} %get-tuple-element.10.nv_ref, bf16[4,2,512,128]{3,2,1,0:T(8,128)(2,1)} %k_ref.1, ...), custom_call_target="tpu_custom_call" | custom-call | tf_op jit(solution)/shard_map/insert/pallas_call | solution.py:301
  70.2 0.0 copy-start
  70.2 0.7 copy-done
  70.9 0.6 copy.18
Async XLA Ops:
  70.2 0.7 copy-start

commit v2 on v1

v2 whole, which is shorter than its diff:
```python
import functools

import jax
import jax.numpy as jnp
from jax import lax
from jax.experimental import pallas as pl
from jax.experimental.pallas import tpu as pltpu
from jax.sharding import PartitionSpec as P

MESH = pl.DeviceIdType.MESH
HBM = pl.BlockSpec(memory_space=pl.ANY)
VMEM = pl.BlockSpec(memory_space=pltpu.VMEM)

D = 4096
NZ, NY, NT = 16, 4, 8
HALF = NZ // 2
SEQS, PROPS, TOKENS = 4, 16, 64
EPS = 1e-06
MASKED = -1e30
HEAD_SCALE = 0.8
F32, BF16 = jnp.float32, jnp.bfloat16
LAST = (((1,), (1,)), ((), ()))
OUT = pltpu.VMEM


def z_step(k):
    odd = lax.rem(k, 2)
    return 8 + odd * lax.div(k + 1, 2) - (1 - odd) * lax.div(k, 2)


def half_step(k):
    odd = lax.rem(k, 2)
    return odd * (19 - lax.div(k, 2)) + (1 - odd) * (12 + lax.div(k, 2))


def to_plane(z, y, steps, step_of, send):
    def far(i, carry):
        send(lax.rem(z + step_of(lax.div(i, NY)), NZ), lax.rem(y + lax.rem(i, NY), NY))
        return carry

    lax.fori_loop(0, steps * NY, far, 0)

    def near(i, carry):
        send(z, lax.rem(y + i, NY))
        return carry

    lax.fori_loop(1, NY, near, 0)


def wait_bytes(ref, count, sem):
    piece = ref.at[pl.ds(0, count)]
    pltpu.make_async_copy(piece, piece, sem).wait()


def split3(x):
    high = x.astype(BF16).astype(F32)
    rest = x - high
    mid = rest.astype(BF16).astype(F32)
    return high, mid, (rest - mid).astype(BF16).astype(F32)


def fused(
    tok_in, gain_in, wq_in, wk_in, wv_in, wo_in, lam_in, sub_in, prior_in, acc_in, par_in, kc_in, vc_in,
    mixed_ref, kbuf, vbuf,
    tok, gain, wq, wk, wv, sub, par, lam, prior, acc, woall,
    part_q, part_n, yb_q, yb_n, zs_q, zs_n, zb_q, zb_n, ag_q, ag_n, ruler_q, ruler_n, rows, news, reach_ref,
    terms, csrc, cb, cterms, asrc, attb, attf,
    load_sem, y_send, y_recv, yn_send, yn_recv, w_send, w_recv, z_send, z_recv, zn_send, zn_recv,
    a_send, a_recv, an_send, an_recv, c_send, c_recv, t_send, t_recv,
):
    kv, tp = lax.axis_index("kv"), lax.axis_index("tp")
    z, y = lax.div(kv, NY), lax.rem(kv, NY)
    mine = y * NZ + z
    low, upper = lax.rem(z, HALF), lax.div(z, HALF)
    length = kbuf.shape[2]

    barrier = pltpu.get_barrier_semaphore()

    def greet(tz, ty):
        pl.semaphore_signal(barrier, inc=1, device_id=(tz * NY + ty, tp), device_id_type=MESH)

    to_plane(z, y, NZ - 1, z_step, greet)

    def greet_tp(i, carry):
        pl.semaphore_signal(barrier, inc=1, device_id=(kv, lax.rem(tp + i, NT)), device_id_type=MESH)
        return carry

    lax.fori_loop(1, NT, greet_tp, 0)

    pairs = (
        (tok_in, tok), (gain_in, gain), (wq_in, wq), (wk_in, wk), (wv_in, wv), (par_in, par), (wo_in, woall.at[tp]),
        (sub_in, sub), (lam_in, lam), (prior_in, prior), (acc_in, acc), (kc_in, kbuf), (vc_in, vbuf),
    )
    loads = [pltpu.make_async_copy(a, b, load_sem.at[i]) for i, (a, b) in enumerate(pairs)]
    for load in loads:
        load.start()
    for load in loads[:6]:
        load.wait()

    x = tok[...].astype(F32)
    normed = (x * gain[...]).astype(BF16)
    squares = jnp.sum(x * x, axis=1, keepdims=True)
    for w, out, c in ((wq, part_q, 0), (wk, part_n, 0), (wv, part_n, 2)):
        product = jnp.dot(normed, w[...], preferred_element_type=F32)
        out[:, c, :] = product[:, :128]
        out[:, c + 1, :] = product[:, 128:]
    part_q[:, 2, :] = jnp.broadcast_to(squares, (TOKENS, 128))

    at_i = lax.broadcasted_iota(jnp.int32, (PROPS, PROPS), 0)
    at_j = lax.broadcasted_iota(jnp.int32, (PROPS, PROPS), 1)
    for s in range(SEQS):
        reach = jnp.where((at_i == par[s : s + 1, :]) | (at_i == at_j), 1.0, 0.0)
        for _ in range(4):
            step = reach.astype(BF16)
            reach = jnp.where(jnp.dot(step, step, preferred_element_type=F32) > 0.5, 1.0, 0.0)
        reach_ref[s] = reach

    for load in loads[6:]:
        load.wait()
    pl.semaphore_wait(barrier, NZ * NY - 1 + NT - 1)

    def send_y(part, yb, sends, recvs):
        for step in (2, 1, 3):
            ty = lax.rem(y + step, NY)
            pltpu.make_async_remote_copy(
                part.at[pl.ds(ty * NZ, NZ)], yb.at[y], sends, recvs, device_id=(z * NY + ty, tp), device_id_type=MESH
            ).start()

    def send_z(zs, zb, sends, recvs):
        def one(k, carry):
            tz = lax.rem(z + z_step(k), NZ)
            pltpu.make_async_remote_copy(
                zs.at[:, lax.rem(tz, HALF)], zb.at[z], sends, recvs, device_id=(tz * NY + y, tp), device_id_type=MESH
            ).start()
            return carry

        lax.fori_loop(0, NZ - 1, one, 0)

    def send_rows(ag, sends, recvs):
        def one(tz, ty):
            piece = ag.at[y, :, low]
            pltpu.make_async_remote_copy(
                piece, piece, sends, recvs, device_id=(tz * NY + ty, tp), device_id_type=MESH
            ).start()

        to_plane(z, y, HALF - 1, half_step, one)

    send_y(part_q, yb_q, y_send, y_recv)
    send_y(part_n, yb_n, yn_send, yn_recv)

    def send_w(i, carry):
        pltpu.make_async_remote_copy(
            woall.at[tp], woall.at[tp], w_send, w_recv, device_id=(kv, lax.rem(tp + i, NT)), device_id_type=MESH
        ).start()
        return carry

    lax.fori_loop(1, NT, send_w, 0)

    for part, yb, recvs, zs, zb, z_sends, z_recvs in (
        (part_q, yb_q, y_recv, zs_q, zb_q, z_send, z_recv),
        (part_n, yb_n, yn_recv, zs_n, zb_n, zn_send, zn_recv),
    ):
        yb[y] = part[pl.ds(y * NZ, NZ)]
        wait_bytes(yb, NY - 1, recvs)
        zs[...] = ((yb[0] + yb[1]) + (yb[2] + yb[3])).reshape(zs.shape)
        send_z(zs, zb, z_sends, z_recvs)
        zb[z] = zs[:, low]

    wait_bytes(zb_q, NZ - 1, z_recv)
    total = jnp.sum(zb_q[...], axis=0)
    scale = lax.rsqrt(total[:, 2:3, :] / D + EPS)
    ag_q[y, :, low] = (total[:, :2, :] * scale).astype(BF16)
    send_rows(ag_q, a_send, a_recv)
    wait_bytes(zb_n, NZ - 1, zn_recv)
    ag_n[y, :, low] = (jnp.sum(zb_n[...], axis=0) * scale).astype(BF16)
    send_rows(ag_n, an_send, an_recv)

    wait_bytes(ruler_q, TOKENS - 2, a_recv)
    rows[...] = ag_q[...].astype(F32).reshape(rows.shape)
    lane = lax.broadcasted_iota(jnp.int32, (PROPS, 128), 1)
    position = lax.broadcasted_iota(jnp.int32, (2 * PROPS, length), 1) + kv * length
    for s in range(SEQS):
        settled = position < prior[s] + acc[s]
        tokens = slice(s * PROPS, (s + 1) * PROPS)
        stats = jnp.zeros((PROPS, 128), F32)
        for h in range(2):
            q = rows[tokens, h, :]
            both = jnp.concatenate([jnp.where(lane < 64, q, 0.0), jnp.where(lane < 64, 0.0, q)], axis=0).astype(BF16)
            scores = lax.dot_general(both, kbuf[s, h], LAST, preferred_element_type=F32) * 0.125
            maximum = jnp.max(jnp.where(settled, scores, MASKED), axis=1, keepdims=True)
            weight = jnp.where(settled, jnp.exp(scores - maximum), 0.0)
            totals = jnp.sum(weight, axis=1, keepdims=True)
            summed = jnp.dot(weight.astype(BF16), vbuf[s, h], preferred_element_type=F32)
            for m in range(2):
                c = 2 * m + h
                half = slice(m * PROPS, (m + 1) * PROPS)
                terms[tokens, c, :] = summed[half]
                for n, column in ((c, maximum[half]), (4 + c, totals[half])):
                    for k, piece in enumerate(split3(column)):
                        stats = jnp.where(lane == 8 * k + n, piece, stats)
        terms[tokens, 4, :] = stats
        terms[tokens, 5, :] = jnp.zeros((PROPS, 128), F32)
    csrc[...] = terms[...].astype(BF16)

    def send_c(tz, ty):
        pltpu.make_async_remote_copy(
            csrc.at[ty * NZ + tz], cb.at[mine], c_send, c_recv, device_id=(tz * NY + ty, tp), device_id_type=MESH
        ).start()

    to_plane(z, y, NZ - 1, z_step, send_c)
    cb[mine] = csrc[mine]

    wait_bytes(ruler_n, TOKENS - 2, an_recv)
    news[...] = ag_n[...].astype(F32).reshape(news.shape)
    own_q = ag_q[y, upper, low].astype(F32)
    family = pl.ds(y * PROPS, PROPS)
    related = jnp.sum(jnp.where(at_j == z, reach_ref[y], 0.0), axis=1, keepdims=True) > 0.5
    tree = []
    for m in range(2):
        for h in range(2):
            product = own_q[h : h + 1, :] * news[family, h, :]
            mine_only = lane < 64 if m == 0 else lane >= 64
            scores = jnp.sum(jnp.where(mine_only, product, 0.0), axis=1, keepdims=True) * 0.125
            maximum = jnp.max(jnp.where(related, scores, MASKED), axis=0, keepdims=True)
            weight = jnp.where(related, jnp.exp(scores - maximum), 0.0)
            summed = jnp.sum(weight.astype(BF16).astype(F32) * news[family, 2 + h, :], axis=0, keepdims=True)
            tree.append((maximum, jnp.sum(weight, axis=0, keepdims=True), summed))

    offset = lax.broadcasted_iota(jnp.int32, (length, PROPS), 0) + kv * length
    column = lax.broadcasted_iota(jnp.int32, (length, PROPS), 1)
    across = lax.broadcasted_iota(jnp.int32, (length, 128), 0) + kv * length
    for s in range(SEQS):
        end = prior[s] + acc[s]
        hot = jnp.where(offset - end == column, 1.0, 0.0).astype(BF16)
        inside = (across >= end) & (across < end + PROPS)
        for h in range(2):
            for buf, c in ((kbuf, h), (vbuf, 2 + h)):
                new = news[s * PROPS : (s + 1) * PROPS, c, :].astype(BF16)
                placed = jnp.dot(hot, new, preferred_element_type=F32)
                buf[s, h] = jnp.where(inside, placed, buf[s, h].astype(F32)).astype(BF16)

    wait_bytes(cb, NZ * NY - 1, c_recv)
    cterms[...] = cb[...].astype(F32)
    st = cterms[:, 4, :]
    heads = []
    for c in range(4):
        tree_max, tree_total, tree_summed = tree[c]
        maxima = (st[:, c : c + 1] + st[:, 8 + c : 9 + c]) + st[:, 16 + c : 17 + c]
        shares = (st[:, 4 + c : 5 + c] + st[:, 12 + c : 13 + c]) + st[:, 20 + c : 21 + c]
        largest = jnp.maximum(jnp.max(maxima, axis=0, keepdims=True), tree_max)
        factor, tree_factor = jnp.exp(maxima - largest), jnp.exp(tree_max - largest)
        whole = jnp.sum(factor * shares, axis=0, keepdims=True) + tree_factor * tree_total
        summed = jnp.sum(factor * cterms[:, c, :], axis=0, keepdims=True) + tree_factor * tree_summed
        heads.append(summed / whole)
    attended = []
    for h in range(2):
        head_out = heads[h] - lam[h] * heads[2 + h]
        square = jnp.mean(head_out * head_out, axis=1, keepdims=True)
        attended.append(head_out * lax.rsqrt(square + EPS) * sub[...] * HEAD_SCALE)
    done = jnp.concatenate(attended, axis=0).astype(BF16)
    asrc[...] = done

    target = 2 * y + upper

    def send_t(tz, ty):
        pltpu.make_async_remote_copy(
            asrc, attb.at[tp, low], t_send, t_recv, device_id=(tz * NY + ty, target), device_id_type=MESH
        ).start()

    to_plane(z, y, NZ - 1, z_step, send_t)

    @pl.when(target == tp)
    def _():
        attb[tp, low] = done
        wait_bytes(ruler_q, TOKENS - 1, t_recv)
        wait_bytes(ruler_q, TOKENS - 1, t_send)

    @pl.when(target != tp)
    def _():
        send_t(z, y)
        wait_bytes(ruler_q, TOKENS, t_recv)
        wait_bytes(ruler_q, TOKENS, t_send)

    wait_bytes(woall, NT - 1, w_recv)

    attf[...] = attb[...].astype(F32).reshape(attf.shape)
    mixed = jnp.zeros(mixed_ref.shape, F32)
    for g in range(NT):
        group = slice(g * 8, (g + 1) * 8)
        product = lax.dot_general(
            attf[group, 0, :].astype(BF16), woall[g, :, :128], LAST, preferred_element_type=F32
        ) + lax.dot_general(attf[group, 1, :].astype(BF16), woall[g, :, 128:], LAST, preferred_element_type=F32)
        mixed += product.astype(BF16).astype(F32)
    mixed_ref[...] = mixed.astype(BF16)

    wait_bytes(yb_q, NY - 1, y_send)
    wait_bytes(yb_n, NY - 1, yn_send)
    wait_bytes(woall, NT - 1, w_send)
    wait_bytes(zb_q, NZ - 1, z_send)
    wait_bytes(zb_n, NZ - 1, zn_send)
    wait_bytes(ruler_q, TOKENS - 2, a_send)
    wait_bytes(ruler_n, TOKENS - 2, an_send)
    wait_bytes(cb, NZ * NY - 1, c_send)


def body(
    tokens, norm_gain, w_query, w_key, w_value, w_out, lambdas, sub_gain, key_cache, value_cache, prior, accepted, parent
):
    length = key_cache.shape[2]
    return pl.pallas_call(
        fused,
        name="fused",
        out_shape=(
            OUT((TOKENS // NT, 64), BF16),
            OUT(key_cache.shape, BF16),
            OUT(value_cache.shape, BF16),
        ),
        in_specs=[HBM] * 13,
        out_specs=(VMEM,) * 3,
        scratch_shapes=[
            pltpu.VMEM((TOKENS, 64), BF16),
            pltpu.VMEM((1, 64), F32),
            pltpu.VMEM((64, 256), BF16),
            pltpu.VMEM((64, 256), BF16),
            pltpu.VMEM((64, 256), BF16),
            pltpu.VMEM((1, 128), F32),
            pltpu.VMEM((SEQS, PROPS), jnp.int32),
            pltpu.SMEM((2,), F32),
            pltpu.SMEM((SEQS,), jnp.int32),
            pltpu.SMEM((SEQS,), jnp.int32),
            pltpu.VMEM((NT, 64, 256), BF16),
            pltpu.VMEM((TOKENS, 3, 128), F32),
            pltpu.VMEM((TOKENS, 4, 128), F32),
            pltpu.VMEM((NY, NZ, 3, 128), F32),
            pltpu.VMEM((NY, NZ, 4, 128), F32),
            pltpu.VMEM((2, HALF, 3, 128), F32),
            pltpu.VMEM((2, HALF, 4, 128), F32),
            pltpu.VMEM((NZ, 2, 3, 128), F32),
            pltpu.VMEM((NZ, 2, 4, 128), F32),
            pltpu.VMEM((SEQS, 2, HALF, 2, 128), BF16),
            pltpu.VMEM((SEQS, 2, HALF, 4, 128), BF16),
            pltpu.VMEM((TOKENS, 2, 128), BF16),
            pltpu.VMEM((TOKENS, 4, 128), BF16),
            pltpu.VMEM((TOKENS, 2, 128), F32),
            pltpu.VMEM((TOKENS, 4, 128), F32),
            pltpu.VMEM((SEQS, PROPS, PROPS), F32),
            pltpu.VMEM((TOKENS, 6, 128), F32),
            pltpu.VMEM((TOKENS, 6, 128), BF16),
            pltpu.VMEM((TOKENS, 6, 128), BF16),
            pltpu.VMEM((TOKENS, 6, 128), F32),
            pltpu.VMEM((2, 128), BF16),
            pltpu.VMEM((NT, 8, 2, 128), BF16),
            pltpu.VMEM((TOKENS, 2, 128), F32),
            pltpu.SemaphoreType.DMA((13,)),
        ]
        + [pltpu.SemaphoreType.DMA] * 18,
        compiler_params=pltpu.CompilerParams(collective_id=0, has_side_effects=True),
    )(
        tokens, norm_gain.reshape(1, -1), w_query, w_key, w_value, w_out.T, lambdas, sub_gain.reshape(1, -1),
        prior, accepted, parent, key_cache, value_cache,
    )


def solution(mesh):
    in_specs = (
        P(None, "kv"),
        P("kv"),
        P("kv", "tp"),
        P("kv", "tp"),
        P("kv", "tp"),
        P("tp", "kv"),
        P("tp"),
        P(),
        P(None, "tp", "kv", None),
        P(None, "tp", "kv", None),
        P(),
        P(),
        P(),
    )
    out_specs = (P("tp", "kv"), P(None, "tp", "kv", None), P(None, "tp", "kv", None))
    return jax.shard_map(body, mesh=mesh, in_specs=in_specs, out_specs=out_specs, check_vma=False)
```

time: 71.8 us -> 58.1 us (0.81)
  Pallas kernels: 68 us -> 54.8 us
    pallas_call x2 -> x1, Pallas kernels: 68 us -> 54.8 us  [body(): pl.pallas_call(fused, name='fused', out_shape=(OUT((TOKENS // NT, 64), BF...]
    unnamed x4 -> x3, local copies, waits for them, and re-layouts: 2.75 us -> 2.52 us
where the time goes in v2:
time: 58.1 us; the launch traced here: 58 us
  Pallas kernels  54.8 us (94%)
  local copies, waits for them, and re-layouts  2.52 us (4%)
  between operations  0.64 us (1%)
    pallas_call x1, Pallas kernels, body(): pl.pallas_call(fused, name='fused', out_shape=(OUT((TOKENS // NT, 64), BF...  54.8 us
    unnamed x3, local copies, waits for them, and re-layouts  2.52 us

profile of v2, /device:TPU:1, one launch (start us, length us, event | category | flops | bytes accessed | tf_op | source)
XLA Modules:
  0.0 58.0 jit_solution(13054901469748064548)
XLA Ops:
  0.6 54.8 %fused.1 = (bf16[8,64]{1,0:T(8,128)(2,1)S(1)}, bf16[4,2,512,128]{3,2,1,0:T(8,128)(2,1)S(1)}, bf16[4,2,512,128]{3,2,1,0:T(8,128)(2,1)S(1)}) custom-call(bf16[64,64]{1,0:T(8,128)(2,1)} %tok_in.1, f32[1,64]{1,0:T(1,128)} %bitcast.4, bf16[64,256]{1,0:T(8,128)(2,1)} %wq_in.1, bf16[64,256]{1,0:T(8,128)(2,1)} %wk_in.1, bf16[64,256]{1,0:T(8,128)(2,1)} %wv_in.1, ...), custom_call_target="tpu_custom_call" | custom-call | tf_op jit(solution)/shard_map/fused/pallas_call | solution.py:310
  55.4 0.6 %copy.19 = bf16[8,64]{1,0:T(8,128)(2,1)} copy(bf16[8,64]{1,0:T(8,128)(2,1)S(1)} %get-tuple-element.3) | data formatting | bytes 2048
  56.0 1.0 %copy.20 = bf16[4,2,512,128]{3,2,1,0:T(8,128)(2,1)} copy(bf16[4,2,512,128]{3,2,1,0:T(8,128)(2,1)S(1)} %get-tuple-element.4) | data formatting | bytes 2097152
  57.0 1.0 %copy.21 = bf16[4,2,512,128]{3,2,1,0:T(8,128)(2,1)} copy(bf16[4,2,512,128]{3,2,1,0:T(8,128)(2,1)S(1)} %get-tuple-element.5) | data formatting | bytes 2097152

commit v3 on v2

--- a/solution.py
+++ b/solution.py
@@ -66,7 +66,7 @@
     part_q, part_n, yb_q, yb_n, zs_q, zs_n, zb_q, zb_n, ag_q, ag_n, ruler_q, ruler_n, rows, news, reach_ref,
     terms, csrc, cb, cterms, asrc, attb, attf,
     load_sem, y_send, y_recv, yn_send, yn_recv, w_send, w_recv, z_send, z_recv, zn_send, zn_recv,
-    a_send, a_recv, an_send, an_recv, c_send, c_recv, t_send, t_recv,
+    a_send, a_recv, an_send, an_recv, c_send, c_recv, t_send, t_recv, in_2, in_4, in_8,
 ):
     kv, tp = lax.axis_index("kv"), lax.axis_index("tp")
     z, y = lax.div(kv, NY), lax.rem(kv, NY)
@@ -76,16 +76,15 @@
 
     barrier = pltpu.get_barrier_semaphore()
 
-    def greet(tz, ty):
-        pl.semaphore_signal(barrier, inc=1, device_id=(tz * NY + ty, tp), device_id_type=MESH)
-
-    to_plane(z, y, NZ - 1, z_step, greet)
-
-    def greet_tp(i, carry):
+    def signal_z(step, sem):
+        for tz in (lax.rem(z + step, NZ), lax.rem(z + NZ - step, NZ)):
+            pl.semaphore_signal(sem, inc=1, device_id=(tz * NY + y, tp), device_id_type=MESH)
+
+    signal_z(1, barrier)
+    for i in range(1, NY):
+        pl.semaphore_signal(barrier, inc=1, device_id=(z * NY + lax.rem(y + i, NY), tp), device_id_type=MESH)
+    for i in range(1, NT):
         pl.semaphore_signal(barrier, inc=1, device_id=(kv, lax.rem(tp + i, NT)), device_id_type=MESH)
-        return carry
-
-    lax.fori_loop(1, NT, greet_tp, 0)
 
     pairs = (
         (tok_in, tok), (gain_in, gain), (wq_in, wq), (wk_in, wk), (wv_in, wv), (par_in, par), (wo_in, woall.at[tp]),
@@ -115,9 +114,8 @@
             reach = jnp.where(jnp.dot(step, step, preferred_element_type=F32) > 0.5, 1.0, 0.0)
         reach_ref[s] = reach
 
-    for load in loads[6:]:
-        load.wait()
-    pl.semaphore_wait(barrier, NZ * NY - 1 + NT - 1)
+    pl.semaphore_wait(barrier, 2 + NY - 1 + NT - 1)
+    signal_z(1, in_2)
 
     def send_y(part, yb, sends, recvs):
         for step in (2, 1, 3):
@@ -154,7 +152,14 @@
         ).start()
         return carry
 
+    pl.semaphore_wait(in_2, 2)
+    signal_z(2, in_4)
+    loads[6].wait()
     lax.fori_loop(1, NT, send_w, 0)
+    pl.semaphore_wait(in_4, 2)
+    signal_z(4, in_8)
+    for load in loads[7:]:
+        load.wait()
 
     for part, yb, recvs, zs, zb, z_sends, z_recvs in (
         (part_q, yb_q, y_recv, zs_q, zb_q, z_send, z_recv),
@@ -163,6 +168,8 @@
         yb[y] = part[pl.ds(y * NZ, NZ)]
         wait_bytes(yb, NY - 1, recvs)
         zs[...] = ((yb[0] + yb[1]) + (yb[2] + yb[3])).reshape(zs.shape)
+        if part is part_q:
+            pl.semaphore_wait(in_8, 2)
         send_z(zs, zb, z_sends, z_recvs)
         zb[z] = zs[:, low]
 
@@ -303,11 +310,22 @@
     wait_bytes(cb, NZ * NY - 1, c_send)
 
 
+def copy_out(mixed_ref, k_ref, v_ref, mixed_out, k_out, v_out, sems):
+    copies = [pltpu.make_async_copy(mixed_ref, mixed_out, sems.at[2 * SEQS])]
+    for s in range(SEQS):
+        copies.append(pltpu.make_async_copy(k_ref.at[s], k_out.at[s], sems.at[s]))
+        copies.append(pltpu.make_async_copy(v_ref.at[s], v_out.at[s], sems.at[SEQS + s]))
+    for copy in copies:
+        copy.start()
+    for copy in copies:
+        copy.wait()
+
+
 def body(
     tokens, norm_gain, w_query, w_key, w_value, w_out, lambdas, sub_gain, key_cache, value_cache, prior, accepted, parent
 ):
     length = key_cache.shape[2]
-    return pl.pallas_call(
+    results = pl.pallas_call(
         fused,
         name="fused",
         out_shape=(
@@ -353,12 +371,22 @@
             pltpu.VMEM((TOKENS, 2, 128), F32),
             pltpu.SemaphoreType.DMA((13,)),
         ]
-        + [pltpu.SemaphoreType.DMA] * 18,
+        + [pltpu.SemaphoreType.DMA] * 18
+        + [pltpu.SemaphoreType.REGULAR] * 3,
         compiler_params=pltpu.CompilerParams(collective_id=0, has_side_effects=True),
     )(
         tokens, norm_gain.reshape(1, -1), w_query, w_key, w_value, w_out.T, lambdas, sub_gain.reshape(1, -1),
         prior, accepted, parent, key_cache, value_cache,
     )
+    return pl.pallas_call(
+        copy_out,
+        name="copy_out",
+        out_shape=tuple(jax.ShapeDtypeStruct(r.shape, r.dtype) for r in results),
+        in_specs=[VMEM] * 3,
+        out_specs=(HBM,) * 3,
+        scratch_shapes=[pltpu.SemaphoreType.DMA((2 * SEQS + 1,))],
+        compiler_params=pltpu.CompilerParams(vmem_limit_bytes=1 << 20),
+    )(*results)
 
 
 def solution(mesh):

time: 58.1 us -> 55.5 us (0.955)
  local copies, waits for them, and re-layouts: 2.52 us -> 0 us
    unnamed x3 -> x0, local copies, waits for them, and re-layouts: 2.52 us -> none
    pallas_call x1, Pallas kernels: 54.8 us -> 53.3 us  [body(): pl.pallas_call(fused, name='fused', out_shape=(OUT((TOKENS // NT, 64), BF...]
    pallas_call x0 -> x1, Pallas kernels: none -> 1.39 us  [body(): pl.pallas_call(copy_out, name='copy_out', out_shape=tuple((jax.ShapeDtype...]
where the time goes in v3:
time: 55.5 us; the launch traced here: 55.3 us
  Pallas kernels  54.6 us (98%)
  between operations  0.64 us (1%)
    pallas_call x1, Pallas kernels, body(): pl.pallas_call(fused, name='fused', out_shape=(OUT((TOKENS // NT, 64), BF...  53.3 us
    pallas_call x1, Pallas kernels, body(): pl.pallas_call(copy_out, name='copy_out', out_shape=tuple((jax.ShapeDtype...  1.39 us

profile of v3, /device:TPU:1, one launch (start us, length us, event | category | flops | bytes accessed | tf_op | source)
XLA Modules:
  0.0 55.3 jit_solution(17258686606996993705)
XLA Ops:
  0.6 53.3 %fused.1 = (bf16[8,64]{1,0:T(8,128)(2,1)S(1)}, bf16[4,2,512,128]{3,2,1,0:T(8,128)(2,1)S(1)}, bf16[4,2,512,128]{3,2,1,0:T(8,128)(2,1)S(1)}) custom-call(bf16[64,64]{1,0:T(8,128)(2,1)} %tok_in.1, f32[1,64]{1,0:T(1,128)} %bitcast.4, bf16[64,256]{1,0:T(8,128)(2,1)} %wq_in.1, bf16[64,256]{1,0:T(8,128)(2,1)} %wk_in.1, bf16[64,256]{1,0:T(8,128)(2,1)} %wv_in.1, ...), custom_call_target="tpu_custom_call" | custom-call | tf_op jit(solution)/shard_map/fused/pallas_call | solution.py:328
  53.9 1.4 %copy_out.1 = (bf16[8,64]{1,0:T(8,128)(2,1)}, bf16[4,2,512,128]{3,2,1,0:T(8,128)(2,1)}, bf16[4,2,512,128]{3,2,1,0:T(8,128)(2,1)}) custom-call(bf16[8,64]{1,0:T(8,128)(2,1)S(1)} %get-tuple-element.6.mixed_ref, bf16[4,2,512,128]{3,2,1,0:T(8,128)(2,1)S(1)} %get-tuple-element.7.k_ref, bf16[4,2,512,128]{3,2,1,0:T(8,128)(2,1)S(1)} %get-tuple-element.8.v_ref), custom_call_target="tpu_custom_call" | custom-call | tf_op jit(solution)/shard_map/copy_out/pallas_call | solution.py:381

commit v4 on v3

--- a/solution.py
+++ b/solution.py
@@ -14,6 +14,7 @@
 D = 4096
 NZ, NY, NT = 16, 4, 8
 HALF = NZ // 2
+NEAR = NZ // 4
 SEQS, PROPS, TOKENS = 4, 16, 64
 EPS = 1e-06
 MASKED = -1e30
@@ -66,7 +67,7 @@
     part_q, part_n, yb_q, yb_n, zs_q, zs_n, zb_q, zb_n, ag_q, ag_n, ruler_q, ruler_n, rows, news, reach_ref,
     terms, csrc, cb, cterms, asrc, attb, attf,
     load_sem, y_send, y_recv, yn_send, yn_recv, w_send, w_recv, z_send, z_recv, zn_send, zn_recv,
-    a_send, a_recv, an_send, an_recv, c_send, c_recv, t_send, t_recv, in_2, in_4, in_8,
+    a_send, a_recv, an_send, an_recv, c_send, c_recv, t_send, t_recv, entered,
 ):
     kv, tp = lax.axis_index("kv"), lax.axis_index("tp")
     z, y = lax.div(kv, NY), lax.rem(kv, NY)
@@ -80,7 +81,8 @@
         for tz in (lax.rem(z + step, NZ), lax.rem(z + NZ - step, NZ)):
             pl.semaphore_signal(sem, inc=1, device_id=(tz * NY + y, tp), device_id_type=MESH)
 
-    signal_z(1, barrier)
+    for step in range(NEAR, 0, -1):
+        signal_z(step, barrier)
     for i in range(1, NY):
         pl.semaphore_signal(barrier, inc=1, device_id=(z * NY + lax.rem(y + i, NY), tp), device_id_type=MESH)
     for i in range(1, NT):
@@ -114,8 +116,8 @@
             reach = jnp.where(jnp.dot(step, step, preferred_element_type=F32) > 0.5, 1.0, 0.0)
         reach_ref[s] = reach
 
-    pl.semaphore_wait(barrier, 2 + NY - 1 + NT - 1)
-    signal_z(1, in_2)
+    pl.semaphore_wait(barrier, 2 * NEAR + NY - 1 + NT - 1)
+    signal_z(NEAR, entered)
 
     def send_y(part, yb, sends, recvs):
         for step in (2, 1, 3):
@@ -152,12 +154,8 @@
         ).start()
         return carry
 
-    pl.semaphore_wait(in_2, 2)
-    signal_z(2, in_4)
     loads[6].wait()
     lax.fori_loop(1, NT, send_w, 0)
-    pl.semaphore_wait(in_4, 2)
-    signal_z(4, in_8)
     for load in loads[7:]:
         load.wait()
 
@@ -169,7 +167,7 @@
         wait_bytes(yb, NY - 1, recvs)
         zs[...] = ((yb[0] + yb[1]) + (yb[2] + yb[3])).reshape(zs.shape)
         if part is part_q:
-            pl.semaphore_wait(in_8, 2)
+            pl.semaphore_wait(entered, 2)
         send_z(zs, zb, z_sends, z_recvs)
         zb[z] = zs[:, low]
 
@@ -372,7 +370,7 @@
             pltpu.SemaphoreType.DMA((13,)),
         ]
         + [pltpu.SemaphoreType.DMA] * 18
-        + [pltpu.SemaphoreType.REGULAR] * 3,
+        + [pltpu.SemaphoreType.REGULAR],
         compiler_params=pltpu.CompilerParams(collective_id=0, has_side_effects=True),
     )(
         tokens, norm_gain.reshape(1, -1), w_query, w_key, w_value, w_out.T, lambdas, sub_gain.reshape(1, -1),

time: 55.5 us -> 54.1 us (0.975)
  Pallas kernels: 54.6 us -> 53.3 us
    pallas_call x1, Pallas kernels: 53.3 us -> 51.9 us  [body(): pl.pallas_call(fused, name='fused', out_shape=(OUT((TOKENS // NT, 64), BF...]
where the time goes in v4:
time: 54.1 us; the launch traced here: 53.9 us
  Pallas kernels  53.3 us (99%)
  between operations  0.64 us (1%)
    pallas_call x1, Pallas kernels, body(): pl.pallas_call(fused, name='fused', out_shape=(OUT((TOKENS // NT, 64), BF...  51.9 us
    pallas_call x1, Pallas kernels, body(): pl.pallas_call(copy_out, name='copy_out', out_shape=tuple((jax.ShapeDtype...  1.39 us

profile of v4, /device:TPU:1, one launch (start us, length us, event | category | flops | bytes accessed | tf_op | source)
XLA Modules:
  0.0 53.9 jit_solution(8904209735628341752)
XLA Ops:
  0.6 51.9 %fused.1 = (bf16[8,64]{1,0:T(8,128)(2,1)S(1)}, bf16[4,2,512,128]{3,2,1,0:T(8,128)(2,1)S(1)}, bf16[4,2,512,128]{3,2,1,0:T(8,128)(2,1)S(1)}) custom-call(bf16[64,64]{1,0:T(8,128)(2,1)} %tok_in.1, f32[1,64]{1,0:T(1,128)} %bitcast.4, bf16[64,256]{1,0:T(8,128)(2,1)} %wq_in.1, bf16[64,256]{1,0:T(8,128)(2,1)} %wk_in.1, bf16[64,256]{1,0:T(8,128)(2,1)} %wv_in.1, ...), custom_call_target="tpu_custom_call" | custom-call | tf_op jit(solution)/shard_map/fused/pallas_call | solution.py:326
  52.5 1.4 %copy_out.1 = (bf16[8,64]{1,0:T(8,128)(2,1)}, bf16[4,2,512,128]{3,2,1,0:T(8,128)(2,1)}, bf16[4,2,512,128]{3,2,1,0:T(8,128)(2,1)}) custom-call(bf16[8,64]{1,0:T(8,128)(2,1)S(1)} %get-tuple-element.6.mixed_ref, bf16[4,2,512,128]{3,2,1,0:T(8,128)(2,1)S(1)} %get-tuple-element.7.k_ref, bf16[4,2,512,128]{3,2,1,0:T(8,128)(2,1)S(1)} %get-tuple-element.8.v_ref), custom_call_target="tpu_custom_call" | custom-call | tf_op jit(solution)/shard_map/copy_out/pallas_call | solution.py:379
